TPU v7x, 32 devices: a whole 2x2x4 slice. The times are simulated.
32 devices in a mesh: rep: 2 (over y), fs: 4 (over z), tp: 4 (over x, core).
Axes of the slice: x: 2, y: 2, z: 4, core: 2. Of those that a mesh axis runs over, the one named last changes fastest.
Arguments:
- tokens: bfloat16 [2048, 2048], P(('rep', 'fs')), may hold values from -6 to 6
- gate_weight: bfloat16 [2048, 2816], P('fs', 'tp'), may hold values from -0.125 to 0.125
- up_weight: bfloat16 [2048, 2816], P('fs', 'tp'), may hold values from -0.125 to 0.125
- down_weight: bfloat16 [2816, 2048], P('tp', 'fs'), may hold values from -0.109375 to 0.109375
- out_grad: bfloat16 [2048, 2048], P(('rep', 'fs')), may hold values from -6 to 6
Outputs:
- input_grad: bfloat16 [2048, 2048], P(('rep', 'fs'))
- down_grad: float32 [2816, 2048], P('tp', 'fs')
- row_norms: float32 [2816], P('tp')
All inputs are finite; a program needn't handle non-finite values.
Results may differ from a plain program's by a relative error of at most 0.024.
Values may be sent and summed in bfloat16 or wider, within the bound.
A program may use at most 64 MiB of HBM per device.

v0:
```python
import jax
import jax.numpy as jnp
from jax import lax
from jax.sharding import PartitionSpec as P


def contract_last(left, right):
    return lax.dot_general(
        left, right, (((1,), (1,)), ((), ())), preferred_element_type=jnp.float32
    )


def contract_first(left, right):
    return lax.dot_general(
        left, right, (((0,), (0,)), ((), ())), preferred_element_type=jnp.float32
    )


def on_device(tokens, gate_weight, up_weight, down_weight, out_grad):
    down_full = lax.all_gather(down_weight, "fs", axis=1, tiled=True)
    gate_full, up_full = (
        lax.all_gather(gate_weight, "fs", axis=0, tiled=True),
        lax.all_gather(up_weight, "fs", axis=0, tiled=True),
    )
    gate_pre = jnp.dot(tokens, gate_full, preferred_element_type=jnp.float32)
    up_pre = jnp.dot(tokens, up_full, preferred_element_type=jnp.float32)
    sigma = jax.nn.sigmoid(gate_pre)
    activated = gate_pre * sigma
    hidden = (activated * up_pre).astype(jnp.bfloat16)
    hid_grad = contract_last(out_grad, down_full)
    up_grad = (hid_grad * activated).astype(jnp.bfloat16)
    gate_grad = (hid_grad * up_pre * sigma * (1.0 + gate_pre * (1.0 - sigma))).astype(jnp.bfloat16)
    partial_value = contract_last(gate_grad, gate_full) + contract_last(up_grad, up_full)
    input_grad = lax.psum(partial_value.astype(jnp.bfloat16), "tp")
    columns = lax.all_to_all(out_grad, "fs", split_axis=1, concat_axis=0, tiled=True)
    shard = contract_first(lax.all_gather(hidden, "fs", axis=0, tiled=True), columns)
    shard = lax.psum(shard.astype(jnp.bfloat16), "rep").astype(jnp.float32)
    norms = lax.psum(jnp.sum(shard * shard, axis=1), "fs")
    return (input_grad, shard, norms)


def solution(mesh):
    return jax.shard_map(
        on_device,
        mesh=mesh,
        in_specs=(
            P(("rep", "fs"), None),
            P("fs", "tp"),
            P("fs", "tp"),
            P("tp", "fs"),
            P(("rep", "fs"), None),
        ),
        out_specs=(P(("rep", "fs"), None), P("tp", "fs"), P("tp")),
        check_vma=False,
    )
```

profile of v0, /device:TPU:0, one launch (start us, length us, event | category | flops | bytes accessed | tf_op | source)
XLA Modules:
  0.0 329.1 jit_solution(854777100918134661)
XLA Ops:
  7.2 0.0 copy-start
  7.2 0.0 all-gather.9.cloned.1.call-start
  7.2 0.7 all-gather.9.cloned.1.call-update
  7.9 0.0 all-gather.7.cloned.1.call-start
  8.0 0.7 all-gather.7.cloned.1.call-update
  8.7 0.0 all-gather.5.cloned.1.call-start
  8.7 0.7 all-gather.5.cloned.1.call-update
  9.4 0.0 all-gather.11.cloned.1.call-start
  9.4 62.0 %all-gather.9.cloned.1.call-done = bf16[2048,704]{0,1:T(8,128)(2,1)} async-done(((bf16[512,704]{0,1:T(8,128)(2,1)}), bf16[2048,704]{0,1:T(8,128)(2,1)}) %all-gather.9.cloned.1.call-update) | async-done | bytes 2883600 | tf_op jit(solution)/shard_map/all_gather | solution.py:22
  71.4 0.0 copy-done
  71.4 2.8 fusion.8
  74.2 0.0 copy-start.3
  74.2 0.0 copy-start.2
  74.2 56.6 %all-gather.7.cloned.1.call-done = bf16[2048,704]{0,1:T(8,128)(2,1)} async-done(((bf16[512,704]{0,1:T(8,128)(2,1)}), bf16[2048,704]{0,1:T(8,128)(2,1)}) %all-gather.7.cloned.1.call-update) | async-done | bytes 2883600 | tf_op jit(solution)/shard_map/all_gather | solution.py:23
  130.8 3.7 %multiply_convert_fusion = (bf16[256,704]{0,1:T(8,128)(2,1)}, f32[256,704]{0,1:T(8,128)}) fusion(f32[256,704]{0,1:T(8,128)S(1)} %fusion.8, bf16[256,2048]{1,0:T(8,128)(2,1)S(1)} %copy-done, bf16[2048,704]{0,1:T(8,128)(2,1)} %all-gather.7.cloned.1.call-done), kind=kOutput, calls=%fused_computation.4 | convolution fusion | flops 739278848 | bytes 5734400 | tf_op jit(solution)/shard_map/dot_general | solution.py:26
  134.6 0.0 copy-done.3
  134.6 0.0 all-gather.11.cloned.1.call-update
  134.6 0.0 all-reduce.5.cloned.1.call-start
  134.6 0.0 copy-done.2
  134.7 0.5 copy.8
  135.2 56.6 %all_to_all.19 = bf16[256,4,512]{0,2,1:T(8,128)(2,1)S(1)} all-to-all(bf16[256,4,512]{0,2,1:T(8,128)(2,1)S(1)} %bitcast.14), channel_id=1, replica_groups=mesh['rep'=2,'fs'=4,'tp'=4] {'fs'}, dimensions={1} | all-to-all | bytes 2097152 | tf_op jit(solution)/shard_map/all_to_all | solution.py:35
  191.8 0.5 copy.9
  192.4 17.8 %all-gather.5.cloned.1.call-done = bf16[704,2048]{1,0:T(8,128)(2,1)} async-done(((bf16[704,512]{1,0:T(8,128)(2,1)}), bf16[704,2048]{1,0:T(8,128)(2,1)}) %all-gather.5.cloned.1.call-update) | async-done | bytes 2883600 | tf_op jit(solution)/shard_map/all_gather | solution.py:20
  210.1 3.9 %fusion.7 = f32[256,704]{0,1:T(8,128)} fusion(bf16[256,2048]{1,0:T(8,128)(2,1)} %param.9, bf16[704,2048]{1,0:T(8,128)(2,1)} %all-gather.5.cloned.1.call-done), kind=kOutput, calls=%fused_computation.13 | convolution fusion | flops 738197504 | bytes 4653056 | tf_op jit(solution)/shard_map/dot_general | solution.py:8
  214.1 32.2 %all-gather.11.cloned.1.call-done = bf16[1024,704]{0,1:T(8,128)(2,1)} async-done(((bf16[256,704]{0,1:T(8,128)(2,1)}), bf16[1024,704]{0,1:T(8,128)(2,1)}) %all-gather.11.cloned.1.call-update) | async-done | bytes 1441808 | tf_op jit(solution)/shard_map/all_gather | solution.py:36
  246.3 0.0 copy-start.4
  246.3 3.2 convolution_convert_fusion
  249.5 0.0 all-reduce.5.cloned.1.call-update
  249.5 0.0 all-reduce.3.cloned.1.call-start
  249.6 0.0 copy-done.4
  249.6 0.0 copy-start.1
  249.6 0.0 copy-start.5
  249.6 3.5 %fusion.2 = f32[256,2048]{1,0:T(8,128)S(1)} fusion(bf16[2048,704]{0,1:T(8,128)(2,1)} %all-gather.9.cloned.1.call-done, f32[256,704]{0,1:T(8,128)S(1)} %copy-done.4, f32[256,704]{0,1:T(8,128)} %fusion.7, f32[256,704]{0,1:T(8,128)} %get-tuple-element.6), kind=kOutput, calls=%fused_computation.9 | convolution fusion | flops 739999744 | bytes 7143424 | tf_op jit(solution)/shard_map/dot_general | solution.py:8
  253.1 0.0 copy-done.1
  253.1 0.0 copy-done.5
  253.1 2.0 fusion
  255.2 0.0 all-reduce.3.cloned.1.call-update
  255.2 25.6 %all-reduce.5.cloned.1.call-done = bf16[704,512]{1,0:T(8,128)(2,1)} async-done(((bf16[704,512]{1,0:T(8,128)(2,1)}), bf16[704,512]{1,0:T(8,128)(2,1)}) %all-reduce.5.cloned.1.call-update) | async-done | bytes 720912 | tf_op jit(solution)/shard_map/psum | solution.py:37
  280.8 2.3 multiply_reduce_fusion
  283.1 12.2 %psum.23 = f32[704]{0:T(1024)} all-reduce(f32[704]{0:T(1024)S(1)} %get-tuple-element.3), channel_id=1, replica_groups=mesh['rep'=2,'fs'=4,'tp'=4] {'fs'}, use_global_device_ids=true, to_apply=%region_3.0 | all-reduce | flops 704 | bytes 5632 | tf_op jit(solution)/shard_map/psum | solution.py:38
  295.4 24.5 %all-reduce.3.cloned.1.call-done = bf16[256,2048]{1,0:T(8,128)(2,1)} async-done(((bf16[256,2048]{1,0:T(8,128)(2,1)}), bf16[256,2048]{1,0:T(8,128)(2,1)}) %all-reduce.3.cloned.1.call-update) | async-done | bytes 1048592 | tf_op jit(solution)/shard_map/psum | solution.py:34
  319.9 2.3 copy.12
Async XLA Ops:
  7.2 64.3 %copy-start = (bf16[256,2048]{1,0:T(8,128)(2,1)S(1)}, bf16[256,2048]{1,0:T(8,128)(2,1)}, u32[]{:S(2)}) copy-start(bf16[256,2048]{1,0:T(8,128)(2,1)} %param.5) | copy-start | bytes 3145732
  7.2 64.2 %all-gather.9.cloned.1.call-start = ((), (), s32[]{:S(2)}) async-start(), calls=%async_computation.3 | async-start | bytes 3604480 | tf_op jit(solution)/shard_map/all_gather | solution.py:22
  7.9 122.9 %all-gather.7.cloned.1.call-start = ((), (), s32[]{:S(2)}) async-start(), calls=%async_computation.2 | async-start | bytes 3604480 | tf_op jit(solution)/shard_map/all_gather | solution.py:23
  8.7 201.5 %all-gather.5.cloned.1.call-start = ((), (), s32[]{:S(2)}) async-start(), calls=%async_computation.1 | async-start | bytes 3604480 | tf_op jit(solution)/shard_map/all_gather | solution.py:20
  9.4 236.9 %all-gather.11.cloned.1.call-start = ((), (), s32[]{:S(2)}) async-start(), calls=%async_computation.5 | async-start | bytes 1802240 | tf_op jit(solution)/shard_map/all_gather | solution.py:36
  74.2 60.4 %copy-start.3 = (f32[256,704]{0,1:T(8,128)}, f32[256,704]{0,1:T(8,128)S(1)}, u32[]{:S(2)}) copy-start(f32[256,704]{0,1:T(8,128)S(1)} %fusion.8) | copy-start | bytes 2162692
  74.2 60.4 %copy-start.2 = (bf16[256,2048]{1,0:T(8,128)(2,1)S(1)}, bf16[256,2048]{1,0:T(8,128)(2,1)}, u32[]{:S(2)}) copy-start(bf16[256,2048]{1,0:T(8,128)(2,1)} %param.9) | copy-start | bytes 3145732
  134.6 146.2 %all-reduce.5.cloned.1.call-start = ((), (), s32[]{:S(2)}) async-start(), calls=%async_computation.6 | async-start | bytes 1441792 | tf_op jit(solution)/shard_map/psum | solution.py:37
  246.3 3.3 %copy-start.4 = (f32[256,704]{0,1:T(8,128)S(1)}, f32[256,704]{0,1:T(8,128)}, u32[]{:S(2)}) copy-start(f32[256,704]{0,1:T(8,128)} %copy-done.3) | copy-start | bytes 2162692
  249.5 70.4 %all-reduce.3.cloned.1.call-start = ((), (), s32[]{:S(2)}) async-start(), calls=%async_computation.4 | async-start | bytes 2097152 | tf_op jit(solution)/shard_map/psum | solution.py:34
  249.6 3.5 %copy-start.1 = (bf16[2048,704]{0,1:T(8,128)(2,1)S(1)}, bf16[2048,704]{0,1:T(8,128)(2,1)}, u32[]{:S(2)}) copy-start(bf16[2048,704]{0,1:T(8,128)(2,1)} %all-gather.7.cloned.1.call-done) | copy-start | bytes 8650756
  249.6 3.5 %copy-start.5 = (f32[256,704]{0,1:T(8,128)S(1)}, f32[256,704]{0,1:T(8,128)}, u32[]{:S(2)}) copy-start(f32[256,704]{0,1:T(8,128)} %fusion.7) | copy-start | bytes 2162692
Sparse Core Ops, SparseCore 0:
  9.6 61.8 all-gather.8
  73.0 57.7 all-gather.6
  132.4 77.6 all-gather.4
  211.6 34.6 all-gather.10
  249.6 31.1 all-reduce.4
  283.6 36.2 all-reduce.2
where the time goes:
time: 329 us
  waiting for transfers between devices  221 us (67%)
  blocking collectives  68.9 us (21%)
  matrix products  19.2 us (6%)
  between operations  14.2 us (4%)
  local copies, waits for them, and re-layouts  3.4 us (1%)
    all_gather x1, waiting for transfers between devices, on_device(): lax.all_gather(gate_weight, 'fs', axis=0, tiled=True)  62 us
    all_to_all x1, blocking collectives, on_device(): lax.all_to_all(out_grad, 'fs', split_axis=1, concat_axis=0, tiled=True)  56.6 us
    all_gather x1, waiting for transfers between devices, on_device(): lax.all_gather(up_weight, 'fs', axis=0, tiled=True)  56.6 us
    all_gather x1, waiting for transfers between devices, on_device(): lax.all_gather(hidden, 'fs', axis=0, tiled=True)  32.2 us
    psum x1, waiting for transfers between devices, on_device(): shard = lax.psum(shard.astype(jnp.bfloat16), 'rep').astype(jnp.float32)  25.6 us
    psum x1, waiting for transfers between devices, on_device(): input_grad = lax.psum(partial_value.astype(jnp.bfloat16), 'tp')  24.5 us
    all_gather x1, waiting for transfers between devices, on_device(): down_full = lax.all_gather(down_weight, 'fs', axis=1, tiled=True)  17.8 us
    psum x1, blocking collectives, on_device(): norms = lax.psum(jnp.sum(shard * shard, axis=1), 'fs')  12.2 us
  transfers between devices with their start and end apart: 6, of which 6 were waited for; matrix products, arithmetic and copies ran while one was open for 6% of the time, Pallas kernels for 0%

commit v1 on v0

--- a/solution.py
+++ b/solution.py
@@ -17,7 +17,12 @@
 
 
 def on_device(tokens, gate_weight, up_weight, down_weight, out_grad):
-    down_full = lax.all_gather(down_weight, "fs", axis=1, tiled=True)
+    ring = [down_weight]
+    for hop in range(3):
+        ring.append(lax.ppermute(ring[-1], "fs", [(dev, (dev + 1) % 4) for dev in range(4)]))
+    down_full = jnp.roll(
+        jnp.concatenate(ring[::-1], axis=1), (lax.axis_index("fs") + 1) * ring[0].shape[1], axis=1
+    )
     gate_full, up_full = (
         lax.all_gather(gate_weight, "fs", axis=0, tiled=True),
         lax.all_gather(up_weight, "fs", axis=0, tiled=True),

time: 329 us -> 304 us (0.924)
  blocking collectives: 68.9 us -> 12.2 us
  waiting for transfers between devices: 221 us -> 235 us
  starting transfers between devices: 0.24 us -> 13.4 us
  local copies, waits for them, and re-layouts: 3.4 us -> 11.2 us
    all_to_all x1 -> x0, blocking collectives: 56.6 us -> none  [on_device(): lax.all_to_all(out_grad, 'fs', split_axis=1, concat_axis=0, tiled=True)]
    ppermute x0 -> x3, waiting for transfers between devices: none -> 48.1 us  [on_device(): lax.ppermute(ring[-1], 'fs', [(dev, (dev + 1) % 4) for dev in range(4)])]
    all_gather x1, waiting for transfers between devices: 32.2 us -> 6.82 us  [on_device(): lax.all_gather(hidden, 'fs', axis=0, tiled=True)]
    all_gather x1 -> x0, waiting for transfers between devices: 17.8 us -> none  [on_device(): down_full = lax.all_gather(down_weight, 'fs', axis=1, tiled=True)]
    ppermute x0 -> x3, starting transfers between devices: none -> 9.4 us  [on_device(): lax.ppermute(ring[-1], 'fs', [(dev, (dev + 1) % 4) for dev in range(4)])]
    all_gather x1, waiting for transfers between devices: 62 us -> 71.2 us  [on_device(): lax.all_gather(gate_weight, 'fs', axis=0, tiled=True)]
    unnamed x14 -> x23, local copies, waits for them, and re-layouts: 2.86 us -> 9.82 us
    all_to_all x0 -> x1, starting transfers between devices: none -> 3.86 us  [on_device(): lax.all_to_all(out_grad, 'fs', split_axis=1, concat_axis=0, tiled=True)]
  transfers between devices with their start and end apart: 6 -> 9, of which waited for: 6 -> 7; matrix products, arithmetic and copies ran while one was open for 6% -> 8% of each run, Pallas kernels for 0% -> 0%
where the time goes in v1:
time: 304 us
  waiting for transfers between devices  235 us (77%)
  matrix products  16.1 us (5%)
  between operations  14 us (5%)
  starting transfers between devices  13.4 us (4%)
  blocking collectives  12.2 us (4%)
  local copies, waits for them, and re-layouts  11.2 us (4%)
    all_gather x1, waiting for transfers between devices, on_device(): lax.all_gather(gate_weight, 'fs', axis=0, tiled=True)  71.2 us
    all_gather x1, waiting for transfers between devices, on_device(): lax.all_gather(up_weight, 'fs', axis=0, tiled=True)  56.1 us
    ppermute x3, waiting for transfers between devices, on_device(): lax.ppermute(ring[-1], 'fs', [(dev, (dev + 1) % 4) for dev in range(4)])  48.1 us
    psum x1, waiting for transfers between devices, on_device(): shard = lax.psum(shard.astype(jnp.bfloat16), 'rep').astype(jnp.float32)  26.4 us
    psum x1, waiting for transfers between devices, on_device(): input_grad = lax.psum(partial_value.astype(jnp.bfloat16), 'tp')  24.5 us
    psum x1, blocking collectives, on_device(): norms = lax.psum(jnp.sum(shard * shard, axis=1), 'fs')  12.2 us
    unnamed x23, local copies, waits for them, and re-layouts  9.82 us
    ppermute x3, starting transfers between devices, on_device(): lax.ppermute(ring[-1], 'fs', [(dev, (dev + 1) % 4) for dev in range(4)])  9.4 us
  transfers between devices with their start and end apart: 9, of which 7 were waited for; matrix products, arithmetic and copies ran while one was open for 8% of the time, Pallas kernels for 0%

profile of v1, /device:TPU:0, one launch (start us, length us, event | category | flops | bytes accessed | tf_op | source)
XLA Modules:
  0.0 303.9 jit_solution(18384705678014434820)
XLA Ops:
  7.2 0.0 copy-start
  7.2 0.0 all-gather.6.cloned.1.call-start
  7.2 0.7 all-gather.6.cloned.1.call-update
  7.9 0.0 all-gather.4.cloned.1.call-start
  8.0 0.7 all-gather.4.cloned.1.call-update
  8.7 3.1 %collective-permute-start = (bf16[704,512]{1,0:T(8,128)(2,1)}, bf16[704,512]{1,0:T(8,128)(2,1)S(1)}, u32[]{:S(2)}, u32[]{:S(2)}) collective-permute-start(bf16[704,512]{1,0:T(8,128)(2,1)} %param.8), channel_id=1, source_target_pairs={{0,4},{4,8},{8,12},{12,0},{1,5},{5,9},{9,13},{13,1},{2,6},{6,10},{... | collective-permute-start | bytes 2162696 | tf_op jit(solution)/shard_map/ppermute | solution.py:22
  11.8 2.3 copy.8
  14.0 3.9 %all-to-all-start = ((bf16[256,4,512]{0,2,1:T(8,128)(2,1)}), bf16[256,4,512]{0,2,1:T(8,128)(2,1)S(1)}, u32[]{:S(2)}, u32[]{:S(2)}) async-start(bf16[256,4,512]{0,2,1:T(8,128)(2,1)} %bitcast.1), calls=%async_computation | async-start | bytes 2097152 | tf_op jit(solution)/shard_map/all_to_all | solution.py:40
  17.9 0.0 all-gather.8.cloned.1.call-start
  17.9 19.4 %collective-permute-done = bf16[704,512]{1,0:T(8,128)(2,1)S(1)} collective-permute-done((bf16[704,512]{1,0:T(8,128)(2,1)}, bf16[704,512]{1,0:T(8,128)(2,1)S(1)}, u32[]{:S(2)}, u32[]{:S(2)}) %collective-permute-start) | collective-permute-done | bytes 720928 | tf_op jit(solution)/shard_map/ppermute | solution.py:22
  37.3 6.2 %collective-permute-start.1 = (bf16[704,512]{1,0:T(8,128)(2,1)S(1)}, bf16[704,512]{1,0:T(8,128)(2,1)}, u32[]{:S(2)}, u32[]{:S(2)}) collective-permute-start(bf16[704,512]{1,0:T(8,128)(2,1)S(1)} %collective-permute-done), channel_id=1, source_target_pairs={{0,4},{4,8},{8,12},{12,0},{1,5},{5,9},{9,13},{13,1},{2,6},{6,10},{... | collective-permute-start | bytes 2162696 | tf_op jit(solution)/shard_map/ppermute | solution.py:22
  43.5 71.2 %all-gather.6.cloned.1.call-done = bf16[2048,704]{0,1:T(8,128)(2,1)} async-done(((bf16[512,704]{0,1:T(8,128)(2,1)}), bf16[2048,704]{0,1:T(8,128)(2,1)}) %all-gather.6.cloned.1.call-update) | async-done | bytes 2883600 | tf_op jit(solution)/shard_map/all_gather | solution.py:27
  114.7 0.0 copy-done
  114.7 2.8 fusion.13
  117.5 0.0 copy-start.5
  117.5 56.1 %all-gather.4.cloned.1.call-done = bf16[2048,704]{0,1:T(8,128)(2,1)} async-done(((bf16[512,704]{0,1:T(8,128)(2,1)}), bf16[2048,704]{0,1:T(8,128)(2,1)}) %all-gather.4.cloned.1.call-update) | async-done | bytes 2883600 | tf_op jit(solution)/shard_map/all_gather | solution.py:28
  173.7 3.7 %multiply_convert_fusion = (bf16[256,704]{0,1:T(8,128)(2,1)}, f32[256,704]{0,1:T(8,128)}) fusion(f32[256,704]{0,1:T(8,128)S(1)} %fusion.13, bf16[256,2048]{1,0:T(8,128)(2,1)S(1)} %copy-done, bf16[2048,704]{0,1:T(8,128)(2,1)} %all-gather.4.cloned.1.call-done), kind=kOutput, calls=%fused_computation.7 | convolution fusion | flops 739278848 | bytes 5734400 | tf_op jit(solution)/shard_map/dot_general | solution.py:31
  177.4 0.0 copy-done.5
  177.4 0.0 all-gather.8.cloned.1.call-update
  177.4 0.0 all-reduce.5.cloned.1.call-start
  177.5 0.0 collective-permute-done.1
  177.5 0.1 collective-permute-start.2
  177.6 0.0 all-to-all-done
  177.6 0.0 copy-start.2
  177.6 1.3 copy.9
  178.9 28.7 %collective-permute-done.2 = bf16[704,512]{1,0:T(8,128)(2,1)} collective-permute-done((bf16[704,512]{1,0:T(8,128)(2,1)}, bf16[704,512]{1,0:T(8,128)(2,1)}, u32[]{:S(2)}, u32[]{:S(2)}) %collective-permute-start.2) | collective-permute-done | bytes 720928 | tf_op jit(solution)/shard_map/ppermute | solution.py:22
  207.6 1.2 constant_dynamic-update-slice_fusion.7
  208.8 1.2 constant_dynamic-update-slice_fusion.6
  210.0 0.1 constant_dynamic-update-slice_fusion.5
  210.1 0.0 copy-done.2
  210.2 0.1 constant_dynamic-update-slice_fusion.4
  210.3 0.0 copy-start.3
  210.3 1.3 constant_dynamic-update-slice_fusion.3
  211.6 1.2 constant_dynamic-update-slice_fusion.2
  212.8 0.1 constant_dynamic-update-slice_fusion.1
  212.9 0.1 constant_dynamic-update-slice_fusion
  213.0 0.0 copy-done.3
  213.0 0.0 copy-start.4
  213.0 0.9 fusion.3
  214.0 6.8 %all-gather.8.cloned.1.call-done = bf16[1024,704]{0,1:T(8,128)(2,1)} async-done(((bf16[256,704]{0,1:T(8,128)(2,1)}), bf16[1024,704]{0,1:T(8,128)(2,1)}) %all-gather.8.cloned.1.call-update) | async-done | bytes 1441808 | tf_op jit(solution)/shard_map/all_gather | solution.py:41
  220.8 0.0 copy-done.4
  220.8 0.0 copy-start.6
  220.8 3.3 %convolution_convert_fusion = bf16[704,512]{1,0:T(8,128)(2,1)} fusion(bf16[1024,704]{0,1:T(8,128)(2,1)} %all-gather.8.cloned.1.call-done, bf16[1024,512]{1,0:T(8,128)(2,1)S(1)} %bitcast.15), kind=kOutput, calls=%fused_computation.5 | convolution fusion | flops 738557952 | bytes 3211264 | tf_op jit(solution)/shard_map/dot_general | solution.py:14
  224.1 0.0 all-reduce.5.cloned.1.call-update
  224.1 0.0 all-reduce.3.cloned.1.call-start
  224.2 0.0 copy-done.6
  224.2 0.0 copy-start.1
  224.2 3.3 %fusion.7 = f32[256,2048]{1,0:T(8,128)S(1)} fusion(bf16[2048,704]{0,1:T(8,128)(2,1)} %all-gather.6.cloned.1.call-done, f32[256,704]{0,1:T(8,128)S(1)} %copy-done.6, f32[256,704]{0,1:T(8,128)S(1)} %fusion.3, f32[256,704]{0,1:T(8,128)} %get-tuple-element.6), kind=kOutput, calls=%fused_computation.12 | convolution fusion | flops 739999744 | bytes 7143424 | tf_op jit(solution)/shard_map/dot_general | solution.py:8
  227.5 0.0 copy-done.1
  227.5 2.0 fusion.2
  229.5 0.0 all-reduce.3.cloned.1.call-update
  229.6 26.4 %all-reduce.5.cloned.1.call-done = bf16[704,512]{1,0:T(8,128)(2,1)} async-done(((bf16[704,512]{1,0:T(8,128)(2,1)}), bf16[704,512]{1,0:T(8,128)(2,1)}) %all-reduce.5.cloned.1.call-update) | async-done | bytes 720912 | tf_op jit(solution)/shard_map/psum | solution.py:42
  255.9 2.3 multiply_reduce_fusion
  258.3 12.2 %psum.23 = f32[704]{0:T(1024)} all-reduce(f32[704]{0:T(1024)S(1)} %get-tuple-element.3), channel_id=1, replica_groups=mesh['rep'=2,'fs'=4,'tp'=4] {'fs'}, use_global_device_ids=true, to_apply=%region_3.4 | all-reduce | flops 704 | bytes 5632 | tf_op jit(solution)/shard_map/psum | solution.py:43
  270.5 24.5 %all-reduce.3.cloned.1.call-done = bf16[256,2048]{1,0:T(8,128)(2,1)} async-done(((bf16[256,2048]{1,0:T(8,128)(2,1)}), bf16[256,2048]{1,0:T(8,128)(2,1)}) %all-reduce.3.cloned.1.call-update) | async-done | bytes 1048592 | tf_op jit(solution)/shard_map/psum | solution.py:39
  295.0 2.3 copy.19
Async XLA Ops:
  7.2 107.6 %copy-start = (bf16[256,2048]{1,0:T(8,128)(2,1)S(1)}, bf16[256,2048]{1,0:T(8,128)(2,1)}, u32[]{:S(2)}) copy-start(bf16[256,2048]{1,0:T(8,128)(2,1)} %param.5) | copy-start | bytes 3145732
  7.2 107.6 %all-gather.6.cloned.1.call-start = ((), (), s32[]{:S(2)}) async-start(), calls=%async_computation.2 | async-start | bytes 3604480 | tf_op jit(solution)/shard_map/all_gather | solution.py:27
  7.9 165.8 %all-gather.4.cloned.1.call-start = ((), (), s32[]{:S(2)}) async-start(), calls=%async_computation.1 | async-start | bytes 3604480 | tf_op jit(solution)/shard_map/all_gather | solution.py:28
  8.7 28.6 %collective-permute-start = (bf16[704,512]{1,0:T(8,128)(2,1)}, bf16[704,512]{1,0:T(8,128)(2,1)S(1)}, u32[]{:S(2)}, u32[]{:S(2)}) collective-permute-start(bf16[704,512]{1,0:T(8,128)(2,1)} %param.8), channel_id=1, source_target_pairs={{0,4},{4,8},{8,12},{12,0},{1,5},{5,9},{9,13},{13,1},{2,6},{6,10},{... | collective-permute-start | bytes 2162696 | tf_op jit(solution)/shard_map/ppermute | solution.py:22
  14.0 163.6 %all-to-all-start = ((bf16[256,4,512]{0,2,1:T(8,128)(2,1)}), bf16[256,4,512]{0,2,1:T(8,128)(2,1)S(1)}, u32[]{:S(2)}, u32[]{:S(2)}) async-start(bf16[256,4,512]{0,2,1:T(8,128)(2,1)} %bitcast.1), calls=%async_computation | async-start | bytes 2097152 | tf_op jit(solution)/shard_map/all_to_all | solution.py:40
  17.9 202.9 %all-gather.8.cloned.1.call-start = ((), (), s32[]{:S(2)}) async-start(), calls=%async_computation.4 | async-start | bytes 1802240 | tf_op jit(solution)/shard_map/all_gather | solution.py:41
  37.3 140.2 %collective-permute-start.1 = (bf16[704,512]{1,0:T(8,128)(2,1)S(1)}, bf16[704,512]{1,0:T(8,128)(2,1)}, u32[]{:S(2)}, u32[]{:S(2)}) collective-permute-start(bf16[704,512]{1,0:T(8,128)(2,1)S(1)} %collective-permute-done), channel_id=1, source_target_pairs={{0,4},{4,8},{8,12},{12,0},{1,5},{5,9},{9,13},{13,1},{2,6},{6,10},{... | collective-permute-start | bytes 2162696 | tf_op jit(solution)/shard_map/ppermute | solution.py:22
  117.5 59.9 %copy-start.5 = (f32[256,704]{0,1:T(8,128)}, f32[256,704]{0,1:T(8,128)S(1)}, u32[]{:S(2)}) copy-start(f32[256,704]{0,1:T(8,128)S(1)} %fusion.13) | copy-start | bytes 2162692
  177.4 78.5 %all-reduce.5.cloned.1.call-start = ((), (), s32[]{:S(2)}) async-start(), calls=%async_computation.5 | async-start | bytes 1441792 | tf_op jit(solution)/shard_map/psum | solution.py:42
  177.5 30.1 %collective-permute-start.2 = (bf16[704,512]{1,0:T(8,128)(2,1)}, bf16[704,512]{1,0:T(8,128)(2,1)}, u32[]{:S(2)}, u32[]{:S(2)}) collective-permute-start(bf16[704,512]{1,0:T(8,128)(2,1)} %collective-permute-done.1), channel_id=1, source_target_pairs={{0,4},{4,8},{8,12},{12,0},{1,5},{5,9},{9,13},{13,1},{2,6},{6,10},{... | collective-permute-start | bytes 2162696 | tf_op jit(solution)/shard_map/ppermute | solution.py:22
  177.6 32.5 %copy-start.2 = (bf16[704,512]{1,0:T(8,128)(2,1)S(1)}, bf16[704,512]{1,0:T(8,128)(2,1)}, u32[]{:S(2)}) copy-start(bf16[704,512]{1,0:T(8,128)(2,1)} %param.8) | copy-start | bytes 2162692
  210.3 2.8 copy-start.3
  213.0 7.8 %copy-start.4 = (bf16[4,256,512]{2,1,0:T(8,128)(2,1)S(1)}, bf16[4,256,512]{2,1,0:T(8,128)(2,1)}, u32[]{:S(2)}) copy-start(bf16[4,256,512]{2,1,0:T(8,128)(2,1)} %copy.9) | copy-start | bytes 3145732
  220.8 3.4 %copy-start.6 = (f32[256,704]{0,1:T(8,128)S(1)}, f32[256,704]{0,1:T(8,128)}, u32[]{:S(2)}) copy-start(f32[256,704]{0,1:T(8,128)} %copy-done.5) | copy-start | bytes 2162692
  224.1 70.9 %all-reduce.3.cloned.1.call-start = ((), (), s32[]{:S(2)}) async-start(), calls=%async_computation.3 | async-start | bytes 2097152 | tf_op jit(solution)/shard_map/psum | solution.py:39
  224.2 3.3 %copy-start.1 = (bf16[2048,704]{0,1:T(8,128)(2,1)S(1)}, bf16[2048,704]{0,1:T(8,128)(2,1)}, u32[]{:S(2)}) copy-start(bf16[2048,704]{0,1:T(8,128)(2,1)} %all-gather.4.cloned.1.call-done) | copy-start | bytes 8650756
Sparse Core Ops, SparseCore 0:
  9.6 105.1 all-gather.5
  116.3 57.3 all-gather.3
  177.6 43.2 all-gather.7
  224.2 31.6 all-reduce.4
  258.7 36.2 all-reduce.2
